TPU v7x, 32 devices: a whole 2x2x4 slice. The times are simulated.
32 devices in a mesh: sp: 32 (over z, y, x, core), tp: 1.
Axes of the slice: x: 2, y: 2, z: 4, core: 2. Of those that a mesh axis runs over, the one named last changes fastest.
Arguments:
- queries: bfloat16 [4096, 2048], P('sp', 'tp'), may hold values from -6 to 6
- forget_logits: bfloat16 [2, 4096, 2048], P(None, 'sp', 'tp'), may hold values from -7.5 to 7.5
- value_matrix: bfloat16 [4096, 2048], P('sp', 'tp'), may hold values from -6 to 6
- output_gate_logits: bfloat16 [4096, 2048], P('sp', 'tp'), may hold values from -6 to 6
- forget_slack: float32 [2048], P('tp'), may hold values from 0.00012207031 to 0.07
- spike_log_forget: float32 [4096, 16], P('sp', 'tp'), may hold values from -2.8 to 0, as said below
- head_norm_gain: bfloat16 [128], replicated, may hold values from 0.099609375 to 1.8984375
- output_weight: bfloat16 [2048, 2048], P('tp'), may hold values from -0.125 to 0.125
- residual: bfloat16 [4096, 2048], P('sp'), may hold values from -6 to 6
- mixer_norm_gain: bfloat16 [2048], replicated, may hold values from 0.099609375 to 1.8984375
- mixer_gate_weight: bfloat16 [2048, 5632], P('sp', 'tp'), may hold values from -0.125 to 0.125
- mixer_up_weight: bfloat16 [2048, 5632], P('sp', 'tp'), may hold values from -0.125 to 0.125
- mixer_down_weight: bfloat16 [5632, 2048], P('tp', 'sp'), may hold values from -0.078125 to 0.078125
Outputs:
- layer_out: bfloat16 [4096, 2048], P(('sp', 'tp'))
Inputs may be any that keep to these rules, and one draw needn't show every extreme that they name: `spike_log_forget`: zero at all but a few tokens.
All inputs are finite; a program needn't handle non-finite values.
Results may differ from a plain program's by a relative error of at most 0.015.
Values may be sent and summed in bfloat16 or wider, within the bound.
A program may use at most 192 MiB of HBM per device.

v0:
```python
import jax
import jax.numpy as jnp
from jax import lax
from jax.sharding import PartitionSpec as P

BLOCK = 128
NORM_EPS = 1e-06
BEST_PRECISION = lax.Precision.HIGHEST


def entering(array, axis, join, neutral, backward):
    count = lax.axis_size(axis)
    place = lax.axis_index(axis)
    ahead = count - 1 - place if backward else place
    gathered = jax.tree.map(
        lambda a, kind: lax.all_gather(a.astype(kind), axis), array, (jnp.bfloat16, jnp.bfloat16)
    )
    state = jax.tree.map(lambda a, e: jnp.zeros_like(a) + jnp.asarray(e, a.dtype), array, neutral)

    def one(turn, state):
        source = count - 1 - turn if backward else turn
        return join(
            state,
            jax.tree.map(
                lambda a, own: lax.dynamic_index_in_dim(a, source, 0, False).astype(own.dtype),
                gathered,
                array,
            ),
        )

    return lax.fori_loop(0, ahead, one, state)


def rms_scale(entries, gain_vec):
    return (
        entries
        * lax.rsqrt(jnp.mean(entries * entries, axis=-1, keepdims=True) + NORM_EPS)
        * gain_vec.astype(jnp.float32)
    )


def reverse_rows(tensor):
    return jnp.flip(tensor, 0)


def local_sweep(query_f, key_f, decay_f, value_f):
    row_count, heads_present, head_width = query_f.shape
    blocks_count = row_count // BLOCK
    tri_mask = jnp.tril(jnp.ones((BLOCK, BLOCK), bool))

    def to_blocks(tensor):
        return tensor.reshape(blocks_count, BLOCK, heads_present, head_width)

    def advance(carried, segment):
        state_now, offset = carried
        query_seg, key_seg, decay_seg, value_seg = segment
        running = jnp.cumsum(decay_seg, axis=0)
        query_scaled = query_seg * jnp.exp(running)
        key_scaled = key_seg * jnp.exp(-running)
        scores = jnp.einsum("thd,shd->hts", query_scaled, key_scaled, precision=BEST_PRECISION)
        scores = jnp.where(tri_mask[None], scores, 0.0)
        result = jnp.einsum("hts,shv->thv", scores, value_seg, precision=BEST_PRECISION)
        result = result + jnp.einsum(
            "thd,hdv->thv", query_scaled, state_now, precision=BEST_PRECISION
        )
        final_log = running[-1]
        state_next = jnp.exp(final_log)[:, :, None] * state_now + jnp.einsum(
            "shd,shv->hdv",
            key_seg * jnp.exp(final_log[None] - running),
            value_seg,
            precision=BEST_PRECISION,
        )
        reach = query_seg * jnp.exp(running + offset)
        return ((state_next, offset + final_log), (result, reach))

    initial = (
        jnp.zeros((heads_present, head_width, head_width), jnp.float32),
        jnp.zeros((heads_present, head_width), jnp.float32),
    )
    (state_end, offset_end), (results, reaches) = lax.scan(
        advance,
        initial,
        (to_blocks(query_f), to_blocks(key_f), to_blocks(decay_f), to_blocks(value_f)),
    )
    shape_back = (row_count, heads_present, head_width)
    return (
        results.reshape(shape_back),
        reaches.reshape(shape_back),
        state_end,
        jnp.exp(offset_end),
    )


def chain(earlier, latter):
    return (earlier[0] * latter[0], latter[0][..., None] * earlier[1] + latter[1])


def local(
    queries,
    forget_logits,
    value_matrix,
    output_gate_logits,
    forget_slack,
    spike_log_forget,
    head_norm_gain,
    output_weight,
    residual,
    mixer_norm_gain,
    mixer_gate_weight,
    mixer_up_weight,
    mixer_down_weight,
):
    row_count = queries.shape[0]
    heads_present = spike_log_forget.shape[1]
    head_width = queries.shape[1] // heads_present
    query_f = (jax.nn.silu(queries.astype(jnp.float32)) * head_width ** (-0.5)).reshape(
        row_count, heads_present, head_width
    )
    value_f = value_matrix.astype(jnp.float32).reshape(row_count, heads_present, head_width)
    gate_random_key = (forget_slack * jax.nn.sigmoid(-forget_logits.astype(jnp.float32))).reshape(
        2, row_count, heads_present, head_width
    )
    decay_logarithm = jnp.log1p(-gate_random_key) + spike_log_forget[None, :, :, None]
    fore_local, fore_reach, fore_state, fore_total = local_sweep(
        query_f, gate_random_key[0], decay_logarithm[0], value_f
    )
    back_local, back_reach, back_state, back_total = local_sweep(
        reverse_rows(query_f),
        reverse_rows(gate_random_key[1]),
        reverse_rows(decay_logarithm[1]),
        reverse_rows(value_f),
    )
    neutral = (jnp.ones_like(fore_total), jnp.zeros_like(fore_state))
    _, fore_enter = entering((fore_total, fore_state), "sp", chain, neutral, False)
    _, back_enter = entering((back_total, back_state), "sp", chain, neutral, True)
    fore_out = fore_local + jnp.einsum(
        "thd,hdv->thv", fore_reach, fore_enter, precision=BEST_PRECISION
    )
    back_out = back_local + jnp.einsum(
        "thd,hdv->thv", back_reach, back_enter, precision=BEST_PRECISION
    )
    mixture = fore_out + reverse_rows(back_out)
    mixed = (
        rms_scale(mixture, head_norm_gain).reshape(row_count, heads_present * head_width)
        * jax.nn.silu(output_gate_logits.astype(jnp.float32))
    ).astype(jnp.bfloat16)
    part_rows = row_count // lax.axis_size("tp")
    own_start = lax.axis_index("tp") * part_rows
    partial_out = jnp.dot(mixed, output_weight, preferred_element_type=jnp.float32).astype(
        jnp.bfloat16
    )
    mixer_add = lax.psum_scatter(
        lax.optimization_barrier(partial_out).astype(jnp.float32).astype(jnp.bfloat16),
        "tp",
        scatter_dimension=0,
        tiled=True,
    ).astype(jnp.float32)
    own_resid = lax.dynamic_slice_in_dim(residual, own_start, part_rows, 0)
    hidden_state = (own_resid.astype(jnp.float32) + mixer_add).astype(jnp.bfloat16)
    normed_part = rms_scale(hidden_state.astype(jnp.float32), mixer_norm_gain).astype(jnp.bfloat16)
    normed = lax.all_gather(normed_part, "tp", axis=0, tiled=True)
    gate_act = jnp.dot(
        normed,
        lax.all_gather(mixer_gate_weight, "sp", axis=0, tiled=True),
        preferred_element_type=jnp.float32,
    )
    up_act = jnp.dot(
        normed,
        lax.all_gather(mixer_up_weight, "sp", axis=0, tiled=True),
        preferred_element_type=jnp.float32,
    )
    inner = (jax.nn.silu(gate_act) * up_act).astype(jnp.bfloat16)
    lowered = jnp.dot(
        inner,
        lax.all_gather(mixer_down_weight, "sp", axis=1, tiled=True),
        preferred_element_type=jnp.float32,
    )
    lowered_term = lax.optimization_barrier(lowered.astype(jnp.bfloat16)).astype(jnp.float32)
    ffn_add = lax.psum_scatter(
        lowered_term.astype(jnp.bfloat16), "tp", scatter_dimension=0, tiled=True
    ).astype(jnp.float32)
    return (hidden_state.astype(jnp.float32) + ffn_add).astype(jnp.bfloat16)


def solution(mesh):
    placed = (
        P("sp", "tp"),
        P(None, "sp", "tp"),
        P("sp", "tp"),
        P("sp", "tp"),
        P("tp"),
        P("sp", "tp"),
        P(),
        P("tp", None),
        P("sp", None),
        P(),
        P("sp", "tp"),
        P("sp", "tp"),
        P("tp", "sp"),
    )
    return jax.shard_map(
        local, mesh=mesh, in_specs=placed, out_specs=P(("sp", "tp"), None), check_vma=False
    )
```

profile of v0, /device:TPU:0, one launch (start us, length us, event | category | flops | bytes accessed | tf_op | source)
XLA Modules:
  0.0 728.9 jit_solution(13368527805004820737)
XLA Ops:
  6.5 2.4 divide_multiply_fusion
  9.0 1.7 copy.55
  10.7 3.3 bitcast_add_fusion
  14.0 2.3 slice_bitcast_fusion.1
  16.3 2.3 rev.17
  18.5 2.4 fusion.49
  26.6 3.6 exponential_multiply_fusion
  30.2 3.0 fusion.7
  36.1 2.8 bitcast_multiply_fusion
  38.9 2.1 fusion.6
  43.0 44.7 %all_gather.33 = bf16[32,16,128]{2,1,0:T(8,128)(2,1)S(1)} all-gather(bf16[1,16,128]{2,1,0:T(8,128)(2,1)S(1)} %get-tuple-element.230), channel_id=1, replica_groups=mesh['sp'=32,'tp'=1] {'sp'}, dimensions={0}, use_global_device_ids=true | all-gather | bytes 135168 | tf_op jit(solution)/shard_map/all_gather | solution.py:16
  87.7 39.0 %all_gather.30 = bf16[32,16,128]{2,1,0:T(8,128)(2,1)S(1)} all-gather(bf16[1,16,128]{2,1,0:T(8,128)(2,1)S(1)} %get-tuple-element.227), channel_id=1, replica_groups=mesh['sp'=32,'tp'=1] {'sp'}, dimensions={0}, use_global_device_ids=true | all-gather | bytes 135168 | tf_op jit(solution)/shard_map/all_gather | solution.py:16
  126.7 4.0 convolution_select_fusion.1
  132.0 2.8 convolution_select_fusion
  134.8 1.9 convolution_bitcast_fusion.2
  136.7 3.4 fusion.2
  140.1 3.4 fusion.5
  143.5 7.9 %all-gather.16.cloned.1.call-done = bf16[512,128,128]{2,1,0:T(8,128)(2,1)} async-done(((bf16[16,128,128]{2,1,0:T(8,128)(2,1)}), bf16[512,128,128]{2,1,0:T(8,128)(2,1)}) %all-gather.16.cloned.1.call-update) | async-done | bytes 16777232 | tf_op jit(solution)/shard_map/all_gather | solution.py:16
  151.5 49.8 %while.17 = (s32[]{:T(128)}, f32[16,128,128]{2,1,0:T(8,128)S(1)}, s32[]{:T(128)}, bf16[32,16,128]{2,1,0:T(8,128)(2,1)S(1)}, bf16[32,16,128,128]{3,2,1,0:T(8,128)...) while((s32[]{:T(128)}, f32[16,128,128]{2,1,0:T(8,128)S(1)}, s32[]{:T(128)}, ...), condition=%wide.region_5.6_spmd, body=%wide.region_4.5_spmd.sunk | while | flops 788486 | bytes 2642067 | solution.py:31
  151.6 1.5 convert_add_fusion.6
  156.3 1.5 convert_add_fusion.6
  157.9 1.5 convert_add_fusion.6
  159.5 1.5 convert_add_fusion.6
  161.1 1.6 convert_add_fusion.6
  162.7 1.5 convert_add_fusion.6
  167.5 1.5 convert_add_fusion.6
  169.1 1.6 convert_add_fusion.6
  173.9 1.5 convert_add_fusion.6
  175.5 1.5 convert_add_fusion.6
  177.1 1.5 convert_add_fusion.6
  181.9 1.7 convert_add_fusion.6
  185.2 1.5 convert_add_fusion.6
  188.4 1.5 convert_add_fusion.6
  190.0 1.5 convert_add_fusion.6
  193.2 1.5 convert_add_fusion.6
  194.8 1.5 convert_add_fusion.6
  196.4 1.5 convert_add_fusion.6
  198.0 1.5 convert_add_fusion.6
  201.3 4.7 fusion.1
  206.0 9.3 %rev.20 = f32[128,16,128]{0,2,1:T(8,128)} reverse(f32[128,16,128]{0,2,1:T(8,128)} %fusion.1), dimensions={0} | reverse | bytes 2097152 | tf_op jit(solution)/shard_map/jit(_flip)/rev | solution.py:43
  215.3 52.1 %all-gather.14.cloned.1.call-done = bf16[512,128,128]{2,1,0:T(8,128)(2,1)} async-done(((bf16[16,128,128]{2,1,0:T(8,128)(2,1)}), bf16[512,128,128]{2,1,0:T(8,128)(2,1)}) %all-gather.14.cloned.1.call-update) | async-done | bytes 16777232 | tf_op jit(solution)/shard_map/all_gather | solution.py:16
  268.8 3.7 multiply_reduce_fusion
  273.5 5.0 convolution_convert_fusion
  278.9 133.5 %all-gather.8.cloned.1.call-done = bf16[2048,5632]{1,0:T(8,128)(2,1)} async-done(((bf16[64,5632]{1,0:T(8,128)(2,1)}), bf16[2048,5632]{1,0:T(8,128)(2,1)}) %all-gather.8.cloned.1.call-update) | async-done | bytes 23068688 | tf_op jit(solution)/shard_map/all_gather | solution.py:164
  412.4 12.4 %fusion.43 = f32[128,5632]{1,0:T(8,128)} fusion(bf16[2048,5632]{1,0:T(8,128)(2,1)} %all-gather.8.cloned.1.call-done, bf16[128,2048]{1,0:T(8,128)(2,1)S(1)} %get-tuple-element.216, f32[2048]{0:T(1024)S(1)} %convert_element_type.124, f32[128]{0:T(128)S(1)} %add_rsqrt_fusion.1), kind=kOutput, calls=%fused_computation.81 | convolution fusion | flops 2953838592 | bytes 26485248 | tf_op jit(solution)/shard_map/dot_general | solution.py:162
  424.9 132.3 %all-gather.10.cloned.1.call-done = bf16[2048,5632]{1,0:T(8,128)(2,1)} async-done(((bf16[64,5632]{1,0:T(8,128)(2,1)}), bf16[2048,5632]{1,0:T(8,128)(2,1)}) %all-gather.10.cloned.1.call-update) | async-done | bytes 23068688 | tf_op jit(solution)/shard_map/all_gather | solution.py:169
  557.2 144.8 %all-gather.12.cloned.1.call-done = bf16[5632,2048]{0,1:T(8,128)(2,1)} async-done(((bf16[5632,64]{0,1:T(8,128)(2,1)}), bf16[5632,2048]{0,1:T(8,128)(2,1)}) %all-gather.12.cloned.1.call-update) | async-done | bytes 23068688 | tf_op jit(solution)/shard_map/all_gather | solution.py:175
  702.0 19.5 %convolution_convert_fusion.1 = bf16[128,2048]{1,0:T(8,128)(2,1)S(1)} fusion(bf16[5632,2048]{0,1:T(8,128)(2,1)} %all-gather.12.cloned.1.call-done, bf16[2048,5632]{1,0:T(8,128)(2,1)} %all-gather.10.cloned.1.call-done, f32[128,5632]{1,0:T(8,128)} %fusion.43, bf16[128,2048]{1,0:T(8,128)(2,1)S(1)} %get-tuple-element.216, f32[2048]{0:T(1024)S(1)} %convert_element_type.124, ...), kind=kOutput, calls=%fused_computation.7 | convolution fusion | flops 5911216128 | bytes 50078208 | tf_op jit(solution)/shard_map/dot_general | solution.py:173
  (103 shorter events, 34.2 us)
Async XLA Ops:
  6.5 19.5 %copy-start = (bf16[128,2048]{1,0:T(8,128)(2,1)S(1)}, bf16[128,2048]{1,0:T(8,128)(2,1)}, u32[]{:S(2)}) copy-start(bf16[128,2048]{1,0:T(8,128)(2,1)} %param.19) | copy-start | bytes 1572868
  6.5 144.9 %all-gather.16.cloned.1.call-start = ((), (), s32[]{:S(2)}) async-start(), calls=%async_computation.4 | async-start | bytes 17301504 | tf_op jit(solution)/shard_map/all_gather | solution.py:16
  8.9 1.7 copy-start.8
  22.3 2.3 copy-start.6
  26.6 3.7 copy-start.2
  33.3 234.2 %all-gather.14.cloned.1.call-start = ((), (), s32[]{:S(2)}) async-start(), calls=%async_computation.3 | async-start | bytes 17301504 | tf_op jit(solution)/shard_map/all_gather | solution.py:16
  38.9 4.1 copy-start.11
  38.9 4.1 copy-start.9
  41.1 371.3 %all-gather.8.cloned.1.call-start = ((), (), s32[]{:S(2)}) async-start(), calls=%async_computation | async-start | bytes 23789568 | tf_op jit(solution)/shard_map/all_gather | solution.py:164
  41.8 515.4 %all-gather.10.cloned.1.call-start = ((), (), s32[]{:S(2)}) async-start(), calls=%async_computation.1 | async-start | bytes 23789568 | tf_op jit(solution)/shard_map/all_gather | solution.py:169
  42.4 659.6 %all-gather.12.cloned.1.call-start = ((), (), s32[]{:S(2)}) async-start(), calls=%async_computation.2 | async-start | bytes 23789568 | tf_op jit(solution)/shard_map/all_gather | solution.py:175
  126.7 5.3 copy-start.5
  130.8 4.0 copy-start.3
  267.6 1.2 copy-start.4
  272.5 1.0 copy-start.10
  273.5 5.0 copy-start.7
  702.0 20.4 %copy-start.1 = (bf16[128,2048]{1,0:T(8,128)(2,1)S(1)}, bf16[128,2048]{1,0:T(8,128)(2,1)}, u32[]{:S(2)}) copy-start(bf16[128,2048]{1,0:T(8,128)(2,1)} %param.19) | copy-start | bytes 1572868
Sparse Core Ops, SparseCore 0:
  33.4 117.9 all-gather.15
  154.3 113.1 all-gather.13
  270.3 142.0 all-gather.7
  415.1 142.0 all-gather.9
  559.9 142.0 all-gather.11
where the time goes:
time: 732 us; the launch traced here: 729 us
  waiting for transfers between devices  472 us (64%)
  blocking collectives  83.7 us (11%)
  other arithmetic  67.5 us (9%)
  matrix products  67.2 us (9%)
  local copies, waits for them, and re-layouts  23.1 us (3%)
  between operations  13.4 us (2%)
    all_gather x1, waiting for transfers between devices, local(): lax.all_gather(mixer_down_weight, 'sp', axis=1, tiled=True)  145 us
    all_gather x1, waiting for transfers between devices, local(): lax.all_gather(mixer_gate_weight, 'sp', axis=0, tiled=True)  134 us
    all_gather x1, waiting for transfers between devices, local(): lax.all_gather(mixer_up_weight, 'sp', axis=0, tiled=True)  132 us
    all_gather x2, blocking collectives, entering(): lax.all_gather(a.astype(kind), axis)  83.7 us
    all_gather x2, waiting for transfers between devices, entering(): lax.all_gather(a.astype(kind), axis)  60 us
    add x31, other arithmetic, chain(): latter[0][..., None] * earlier[1] + latter[1]  48.1 us
    dot_general x1, matrix products, local(): jnp.dot(inner, lax.all_gather(mixer_down_weight, 'sp', axis=1, tiled=True...  19.5 us
  transfers between devices with their start and end apart: 5, of which 5 were waited for; matrix products, arithmetic and copies ran while one was open for 15% of the time, Pallas kernels for 0%

commit v1 on v0

--- a/solution.py
+++ b/solution.py
@@ -170,10 +170,13 @@
         preferred_element_type=jnp.float32,
     )
     inner = (jax.nn.silu(gate_act) * up_act).astype(jnp.bfloat16)
+
+    def note_the_members_all(array_here, axis_id, d_out):
+        arr_out = jnp.concatenate(lax.all_gather(array_here, axis_id), axis=d_out)
+        return arr_out
+
     lowered = jnp.dot(
-        inner,
-        lax.all_gather(mixer_down_weight, "sp", axis=1, tiled=True),
-        preferred_element_type=jnp.float32,
+        inner, note_the_members_all(mixer_down_weight, "sp", 1), preferred_element_type=jnp.float32
     )
     lowered_term = lax.optimization_barrier(lowered.astype(jnp.bfloat16)).astype(jnp.float32)
     ffn_add = lax.psum_scatter(

time: 732 us -> 757 us (1.034)
  waiting for transfers between devices: 472 us -> 442 us
  local copies, waits for them, and re-layouts: 23.1 us -> 51.7 us
  other arithmetic: 67.5 us -> 86.9 us
    another operation x2, other arithmetic: 3.72 us -> 24.7 us  [advance(): running = jnp.cumsum(decay_seg, axis=0)]
    all_gather x1, waiting for transfers between devices: 134 us -> 114 us  [local(): lax.all_gather(mixer_gate_weight, 'sp', axis=0, tiled=True)]
    unnamed x30 -> x35, local copies, waits for them, and re-layouts: 8.36 us -> 27.1 us
    reshape x0 -> x1, local copies, waits for them, and re-layouts: none -> 14.3 us  [note_the_members_all(): arr_out = jnp.concatenate(lax.all_gather(array_here, axis_id), axis=d_out)]
    all_gather x1, waiting for transfers between devices: 145 us -> 134 us  [note_the_members_all(): arr_out = jnp.concatenate(lax.all_gather(array_here, axis_id), axis=d_out)]
  transfers between devices with their start and end apart: 5 -> 5, of which waited for: 5 -> 5; matrix products, arithmetic and copies ran while one was open for 15% -> 19% of each run, Pallas kernels for 0% -> 0%
where the time goes in v1:
time: 757 us; the launch traced here: 747 us
  waiting for transfers between devices  442 us (58%)
  other arithmetic  86.9 us (11%)
  blocking collectives  84 us (11%)
  matrix products  67.6 us (9%)
  local copies, waits for them, and re-layouts  51.7 us (7%)
  between operations  13.7 us (2%)
    all_gather x1, waiting for transfers between devices, note_the_members_all(): arr_out = jnp.concatenate(lax.all_gather(array_here, axis_id), axis=d_out)  134 us
    all_gather x1, waiting for transfers between devices, local(): lax.all_gather(mixer_up_weight, 'sp', axis=0, tiled=True)  132 us
    all_gather x1, waiting for transfers between devices, local(): lax.all_gather(mixer_gate_weight, 'sp', axis=0, tiled=True)  114 us
    all_gather x2, blocking collectives, entering(): lax.all_gather(a.astype(kind), axis)  84 us
    all_gather x2, waiting for transfers between devices, entering(): lax.all_gather(a.astype(kind), axis)  59.6 us
    add x31, other arithmetic, chain(): latter[0][..., None] * earlier[1] + latter[1]  48 us
    unnamed x35, local copies, waits for them, and re-layouts  27.1 us
    another operation x2, other arithmetic, advance(): running = jnp.cumsum(decay_seg, axis=0)  24.7 us
  transfers between devices with their start and end apart: 5, of which 5 were waited for; matrix products, arithmetic and copies ran while one was open for 19% of the time, Pallas kernels for 0%

profile of v1, /device:TPU:0, one launch (start us, length us, event | category | flops | bytes accessed | tf_op | source)
XLA Modules:
  0.0 747.3 jit_solution(11760159474741531491)
XLA Ops:
  6.5 3.7 divide_multiply_fusion
  10.2 1.7 copy.95
  12.0 1.9 bitcast_add_fusion
  15.4 23.3 %fusion.49 = f32[128,16,128]{2,1,0:T(8,128)S(1)} fusion(f32[128,16,128]{2,1,0:T(8,128)S(1)} %rev.17), kind=kOutput, calls=%fused_computation.95 | output fusion | flops 33292288 | bytes 2097152 | tf_op jit(solution)/shard_map/while/body/eval_jaxpr/jit(cumsum)/reduce_window_sum | solution.py:57
  38.8 3.1 slice_bitcast_fusion.2
  45.0 3.6 exponential_multiply_fusion
  48.7 3.0 fusion.7
  54.5 2.8 bitcast_multiply_fusion
  57.3 2.1 fusion.6
  61.5 44.7 %all_gather.36 = bf16[32,16,128]{2,1,0:T(8,128)(2,1)S(1)} all-gather(bf16[1,16,128]{2,1,0:T(8,128)(2,1)S(1)} %get-tuple-element.230), channel_id=1, replica_groups=mesh['sp'=32,'tp'=1] {'sp'}, dimensions={0}, use_global_device_ids=true | all-gather | bytes 135168 | tf_op jit(solution)/shard_map/all_gather | solution.py:16
  106.1 39.3 %all_gather.33 = bf16[32,16,128]{2,1,0:T(8,128)(2,1)S(1)} all-gather(bf16[1,16,128]{2,1,0:T(8,128)(2,1)S(1)} %get-tuple-element.227), channel_id=1, replica_groups=mesh['sp'=32,'tp'=1] {'sp'}, dimensions={0}, use_global_device_ids=true | all-gather | bytes 135168 | tf_op jit(solution)/shard_map/all_gather | solution.py:16
  145.5 4.0 convolution_select_fusion.1
  150.8 2.8 convolution_select_fusion
  153.5 1.9 convolution_bitcast_fusion.2
  155.4 3.4 fusion.2
  158.9 3.4 fusion.5
  162.3 7.9 %all-gather.15.cloned.1.call-done = bf16[512,128,128]{2,1,0:T(8,128)(2,1)} async-done(((bf16[16,128,128]{2,1,0:T(8,128)(2,1)}), bf16[512,128,128]{2,1,0:T(8,128)(2,1)}) %all-gather.15.cloned.1.call-update) | async-done | bytes 16777232 | tf_op jit(solution)/shard_map/all_gather | solution.py:16
  170.3 49.7 %while.17 = (s32[]{:T(128)}, f32[16,128,128]{2,1,0:T(8,128)S(1)}, s32[]{:T(128)}, bf16[32,16,128]{2,1,0:T(8,128)(2,1)S(1)}, bf16[32,16,128,128]{3,2,1,0:T(8,128)...) while((s32[]{:T(128)}, f32[16,128,128]{2,1,0:T(8,128)S(1)}, s32[]{:T(128)}, ...), condition=%wide.region_5.6_spmd, body=%wide.region_4.5_spmd.sunk | while | flops 788486 | bytes 2642067 | solution.py:31
  170.4 1.5 convert_add_fusion.6
  172.0 1.5 convert_add_fusion.6
  173.6 1.5 convert_add_fusion.6
  175.2 1.5 convert_add_fusion.6
  178.3 1.6 convert_add_fusion.6
  180.0 1.6 convert_add_fusion.6
  184.8 1.5 convert_add_fusion.6
  189.5 1.5 convert_add_fusion.6
  191.1 1.6 convert_add_fusion.6
  192.7 1.5 convert_add_fusion.6
  194.3 1.5 convert_add_fusion.6
  195.9 1.5 convert_add_fusion.6
  197.5 1.5 convert_add_fusion.6
  200.7 1.6 convert_add_fusion.6
  205.5 1.5 convert_add_fusion.6
  208.7 1.5 convert_add_fusion.6
  215.1 1.6 convert_add_fusion.6
  218.3 1.6 convert_add_fusion.6
  220.0 5.0 fusion.1
  225.0 9.3 %rev.20 = f32[128,16,128]{0,2,1:T(8,128)} reverse(f32[128,16,128]{0,2,1:T(8,128)} %fusion.1), dimensions={0} | reverse | bytes 2097152 | tf_op jit(solution)/shard_map/jit(_flip)/rev | solution.py:43
  234.3 51.6 %all-gather.13.cloned.1.call-done = bf16[512,128,128]{2,1,0:T(8,128)(2,1)} async-done(((bf16[16,128,128]{2,1,0:T(8,128)(2,1)}), bf16[512,128,128]{2,1,0:T(8,128)(2,1)}) %all-gather.13.cloned.1.call-update) | async-done | bytes 16777232 | tf_op jit(solution)/shard_map/all_gather | solution.py:16
  286.1 4.0 multiply_reduce_fusion
  291.1 4.8 convolution_convert_fusion
  296.2 134.3 %all-gather.17.cloned.1.call-done = bf16[180224,64]{0,1:T(8,128)(2,1)} async-done(((bf16[5632,64]{0,1:T(8,128)(2,1)}), bf16[180224,64]{0,1:T(8,128)(2,1)}) %all-gather.17.cloned.1.call-update) | async-done | bytes 23068688 | tf_op jit(solution)/shard_map/all_gather | solution.py:175
  430.5 16.6 %copy.98 = bf16[8,8,32,5632]{3,2,1,0:T(8,128)(2,1)S(1)} copy(bf16[8,8,32,5632]{3,1,2,0:T(8,128)(2,1)} %bitcast.112) | data formatting | bytes 46137344
  447.1 14.3 %copy.87 = bf16[5632,32,64]{0,2,1:T(8,128)(2,1)} copy(bf16[5632,32,64]{0,1,2:T(8,128)(2,1)S(1)} %bitcast.111) | data formatting | bytes 46137344 | tf_op jit(solution)/shard_map/reshape | solution.py:175
  461.4 113.9 %all-gather.9.cloned.1.call-done = bf16[2048,5632]{1,0:T(8,128)(2,1)} async-done(((bf16[64,5632]{1,0:T(8,128)(2,1)}), bf16[2048,5632]{1,0:T(8,128)(2,1)}) %all-gather.9.cloned.1.call-update) | async-done | bytes 23068688 | tf_op jit(solution)/shard_map/all_gather | solution.py:164
  575.3 12.4 %fusion.43 = f32[128,5632]{1,0:T(8,128)} fusion(bf16[2048,5632]{1,0:T(8,128)(2,1)} %all-gather.9.cloned.1.call-done, bf16[128,2048]{1,0:T(8,128)(2,1)S(1)} %get-tuple-element.216, f32[2048]{0:T(1024)S(1)} %convert_element_type.124, f32[128]{0:T(128)S(1)} %add_rsqrt_fusion.1), kind=kOutput, calls=%fused_computation.81 | convolution fusion | flops 2953838592 | bytes 26485248 | tf_op jit(solution)/shard_map/dot_general | solution.py:162
  587.8 132.3 %all-gather.11.cloned.1.call-done = bf16[2048,5632]{1,0:T(8,128)(2,1)} async-done(((bf16[64,5632]{1,0:T(8,128)(2,1)}), bf16[2048,5632]{1,0:T(8,128)(2,1)}) %all-gather.11.cloned.1.call-update) | async-done | bytes 23068688 | tf_op jit(solution)/shard_map/all_gather | solution.py:169
  720.1 19.5 %convolution_convert_fusion.1 = bf16[128,2048]{1,0:T(8,128)(2,1)S(1)} fusion(bf16[5632,2048]{0,1:T(8,128)(2,1)} %bitcast.113, bf16[2048,5632]{1,0:T(8,128)(2,1)} %all-gather.11.cloned.1.call-done, f32[128,5632]{1,0:T(8,128)} %fusion.43, bf16[128,2048]{1,0:T(8,128)(2,1)S(1)} %get-tuple-element.216, f32[2048]{0:T(1024)S(1)} %convert_element_type.124, ...), kind=kOutput, calls=%fused_computation.7 | convolution fusion | flops 5911216128 | bytes 50078208 | tf_op jit(solution)/shard_map/dot_general | solution.py:178
  (109 shorter events, 33.4 us)
Async XLA Ops:
  6.5 38.0 %copy-start = (bf16[128,2048]{1,0:T(8,128)(2,1)S(1)}, bf16[128,2048]{1,0:T(8,128)(2,1)}, u32[]{:S(2)}) copy-start(bf16[128,2048]{1,0:T(8,128)(2,1)} %param.19) | copy-start | bytes 1572868
  6.5 163.7 %all-gather.15.cloned.1.call-start = ((), (), s32[]{:S(2)}) async-start(), calls=%async_computation.3 | async-start | bytes 17301504 | tf_op jit(solution)/shard_map/all_gather | solution.py:16
  10.2 1.7 copy-start.10
  14.0 1.3 copy-start.5
  38.8 4.3 copy-start.6
  38.8 4.2 copy-start.8
  45.0 3.7 copy-start.3
  48.7 106.8 %copy-start.2 = (f32[128,16,128]{2,1,0:T(8,128)}, f32[128,16,128]{2,1,0:T(8,128)S(1)}, u32[]{:S(2)}) copy-start(f32[128,16,128]{2,1,0:T(8,128)S(1)} %get-tuple-element.228) | copy-start | bytes 3145732
  51.7 234.2 %all-gather.13.cloned.1.call-start = ((), (), s32[]{:S(2)}) async-start(), calls=%async_computation.2 | async-start | bytes 17301504 | tf_op jit(solution)/shard_map/all_gather | solution.py:16
  57.3 4.1 copy-start.13
  57.3 4.1 copy-start.11
  59.5 371.0 %all-gather.17.cloned.1.call-start = ((), (), s32[]{:S(2)}) async-start(), calls=%async_computation.4 | async-start | bytes 23789568 | tf_op jit(solution)/shard_map/all_gather | solution.py:175
  60.2 515.1 %all-gather.9.cloned.1.call-start = ((), (), s32[]{:S(2)}) async-start(), calls=%async_computation | async-start | bytes 23789568 | tf_op jit(solution)/shard_map/all_gather | solution.py:164
  60.8 659.3 %all-gather.11.cloned.1.call-start = ((), (), s32[]{:S(2)}) async-start(), calls=%async_computation.1 | async-start | bytes 23789568 | tf_op jit(solution)/shard_map/all_gather | solution.py:169
  145.5 5.3 copy-start.7
  149.5 4.0 copy-start.4
  290.1 1.0 copy-start.12
  291.1 4.8 copy-start.9
  720.1 20.4 %copy-start.1 = (bf16[128,2048]{1,0:T(8,128)(2,1)S(1)}, bf16[128,2048]{1,0:T(8,128)(2,1)}, u32[]{:S(2)}) copy-start(bf16[128,2048]{1,0:T(8,128)(2,1)} %param.19) | copy-start | bytes 1572868
Sparse Core Ops, SparseCore 0:
  51.8 118.3 all-gather.14
  173.1 112.7 all-gather.12
  288.8 141.6 all-gather.16
  433.2 142.0 all-gather.8
  578.0 142.0 all-gather.10
